TPU v7x, 32 devices: a whole 2x2x4 slice. The times are simulated.
32 devices in a mesh: fs: 4 (over y, x), tp: 8 (over z, core).
Axes of the slice: x: 2, y: 2, z: 4, core: 2. Of those that a mesh axis runs over, the one named last changes fastest.
Arguments:
- tokens: bfloat16 [1024, 2048], P('fs', 'tp'), may hold values from -60 to 60
- norm_gain: float32 [2048], P('fs'), may hold values from 0.1 to 1.9
- gate_weight: float32 [4, 2048, 4096], P(None, 'fs', 'tp'), may hold values from -0.125 to 0.125
- up_weight: float32 [4, 2048, 4096], P(None, 'fs', 'tp'), may hold values from -0.125 to 0.125
- down_weight: float32 [4, 2048, 4096], P(None, 'fs', 'tp'), may hold values from -0.125 to 0.125
- route: int32 [1024, 2], P('fs'), may hold values from 0 to 3, all different within a row; in each aligned block of 256 rows (0 to 255, 256 to 511, ...) at most 256 rows name the same one
- route_weight: float32 [1024, 2], P('fs'), may hold values from 0.2 to 1
Outputs:
- mixed: bfloat16 [1024, 2048], P('fs', 'tp')
- gate_new: bfloat16 [4, 2048, 4096], P('fs', None, 'tp')
- up_new: bfloat16 [4, 2048, 4096], P('fs', None, 'tp')
- down_new: bfloat16 [4, 2048, 4096], P('fs', None, 'tp')
Inputs may be any that keep to these rules, and one draw needn't show every extreme that they name: `route`: the 2 experts of a row differ. In each aligned block of 256 rows (the tokens of one index of fs) no expert is named by more than 256 rows, a bound that some block reaches.
All inputs are finite; a program needn't handle non-finite values.
Results may differ from a plain program's by a relative error of at most 0.024.
Values may be sent and summed in bfloat16 or wider, within the bound.
A program may use at most 64 MiB of HBM per device.

v0:
```python
import jax
import jax.numpy as jnp
from jax import lax
from jax.sharding import PartitionSpec as P

epsilon = 1e-05


def slot_table(route, block_rows, expert_count):
    pair_ids = route.reshape(-1, block_rows * route.shape[1])
    onehot = (
        pair_ids[:, :, None] == jnp.arange(expert_count, dtype=jnp.int32)[None, None, :]
    ).astype(jnp.int32)
    before = jnp.cumsum(onehot, axis=1) - onehot
    return jnp.sum(before * onehot, axis=2).reshape(route.shape)


def body(tokens, norm_gain, gate_weight, up_weight, down_weight, route, route_weight):
    experts = gate_weight.shape[0]
    tok_rows = tokens.shape[0]
    columns = tokens.shape[1]
    fs_count = lax.axis_size("fs")
    capacity = 4 * tok_rows // fs_count
    gain_col = norm_gain[None, :, None]
    gate_cast = (gate_weight * gain_col).astype(jnp.bfloat16)
    up_cast = (up_weight * gain_col).astype(jnp.bfloat16)
    down_cast = down_weight.astype(jnp.bfloat16)
    gate_new, up_new, down_new = (
        lax.all_to_all(gate_cast, "fs", split_axis=0, concat_axis=1, tiled=True),
        lax.all_to_all(up_cast, "fs", split_axis=0, concat_axis=1, tiled=True),
        lax.all_to_all(down_cast, "fs", split_axis=0, concat_axis=1, tiled=True),
    )
    slot_of = slot_table(route, tok_rows, experts)
    target = route * capacity + slot_of
    slot_lanes = jnp.arange(experts * capacity, dtype=jnp.int32)
    slot_hits = target[:, :, None] == slot_lanes[None, None, :]
    token_iota = jnp.arange(tok_rows, dtype=jnp.int32)[:, None, None]
    lane_token = jnp.sum(jnp.where(slot_hits, token_iota + 1, 0), axis=(0, 1)) - 1
    lane_token = jnp.where(lane_token < 0, tok_rows, lane_token)
    combine = jnp.sum(jnp.where(slot_hits, route_weight[:, :, None], 0.0), axis=1)
    tok_float = tokens.astype(jnp.float32)
    square_sum = lax.psum(jnp.sum(tok_float * tok_float, axis=1), "tp")
    full_width = columns * lax.axis_size("tp")
    normed = (tok_float * lax.rsqrt(square_sum / full_width + epsilon)[:, None]).astype(
        jnp.bfloat16
    )
    padded = jnp.concatenate([normed, jnp.zeros((1, columns), jnp.bfloat16)], axis=0)
    outgoing = padded[lane_token].reshape(experts, capacity, columns)
    arrived = lax.all_to_all(outgoing, "fs", split_axis=0, concat_axis=0, tiled=True).reshape(
        -1, columns
    )
    gate_local = gate_new[0]
    up_local = up_new[0]
    piece_rows = lax.all_gather(arrived, "tp", axis=1, tiled=True)
    gate_acc = jnp.dot(piece_rows, gate_local, preferred_element_type=jnp.float32)
    up_acc = jnp.dot(piece_rows, up_local, preferred_element_type=jnp.float32)
    hidden = (jax.nn.silu(gate_acc) * up_acc).astype(jnp.bfloat16)
    down_local = down_new[0]
    summed = lax.psum_scatter(
        lax.dot_general(
            down_local, hidden, (((1,), (1,)), ((), ())), preferred_element_type=jnp.float32
        ).astype(jnp.bfloat16),
        "tp",
        scatter_dimension=0,
        tiled=True,
    ).astype(jnp.float32)
    own_columns = summed.shape[0]
    outgoing_back = summed.astype(jnp.bfloat16).reshape(own_columns, fs_count, capacity)
    returned = lax.all_to_all(outgoing_back, "fs", split_axis=1, concat_axis=1, tiled=True).reshape(
        own_columns, experts * capacity
    )
    mixed = lax.dot_general(
        combine,
        returned.astype(jnp.float32),
        (((1,), (1,)), ((), ())),
        precision=lax.Precision.HIGHEST,
        preferred_element_type=jnp.float32,
    )
    return (mixed.astype(jnp.bfloat16), gate_new, up_new, down_new)


def solution(mesh):
    in_specs = (
        P("fs", "tp"),
        P("fs"),
        P(None, "fs", "tp"),
        P(None, "fs", "tp"),
        P(None, "fs", "tp"),
        P("fs", None),
        P("fs", None),
    )
    out_specs = (P("fs", "tp"), P("fs", None, "tp"), P("fs", None, "tp"), P("fs", None, "tp"))
    return jax.shard_map(body, mesh=mesh, in_specs=in_specs, out_specs=out_specs, check_vma=False)
```

profile of v0, /device:TPU:0, one launch (start us, length us, event | category | flops | bytes accessed | tf_op | source)
XLA Modules:
  0.0 224.2 jit_solution(16390866846317587679)
XLA Ops:
  7.2 0.8 copy.21
  8.0 0.1 eq.40
  8.2 1.2 reduce-window.6
  9.4 0.2 slice_reduce_fusion
  9.7 0.2 reduce-window.9
  9.9 0.1 broadcast.105
  10.0 0.1 reshape.192
  10.1 0.1 copy.22
  10.2 0.7 multiply_add_fusion
  10.9 0.3 select_reduce_fusion
  11.2 1.0 fusion
  12.2 18.1 %psum.7 = f32[256]{0:T(256)S(1)} all-reduce(f32[256]{0:T(256)S(1)} %fusion), channel_id=1, replica_groups=mesh['fs'=4,'tp'=8] {'tp'}, use_global_device_ids=true, to_apply=%region_5.6 | all-reduce | flops 256 | bytes 2048 | tf_op jit(solution)/shard_map/psum | solution.py:42
  30.4 1.0 fusion.1
  31.4 3.9 %gather_fusion = bf16[1024,256]{1,0:T(8,128)(2,1)S(1)} fusion(bf16[257,256]{1,0:T(8,128)(2,1)S(1)} %concatenate.3, s32[1024]{0:T(1024)S(1)} %broadcast_clamp_fusion), kind=kCustom, calls=%fused_computation | custom fusion | bytes 1052672 | tf_op jit(solution)/shard_map/gather | solution.py:48
  35.3 10.7 %all_to_all.46 = bf16[4,256,256]{2,1,0:T(8,128)(2,1)} all-to-all(bf16[4,256,256]{2,1,0:T(8,128)(2,1)S(1)} %bitcast.31), channel_id=1, replica_groups=mesh['fs'=4,'tp'=8] {'fs'}, dimensions={0} | all-to-all | bytes 1048576 | tf_op jit(solution)/shard_map/all_to_all | solution.py:49
  46.1 6.1 %multiply_convert_fusion = (bf16[4,512,512]{2,1,0:T(8,128)(2,1)}, bf16[4,512,512]{2,1,0:T(8,128)(2,1)S(1)}) fusion(f32[4,512,512]{2,1,0:T(8,128)} %param.10, f32[512]{0:T(512)S(1)} %copy-done.1, f32[4,512,512]{2,1,0:T(8,128)} %param.9), kind=kLoop, calls=%fused_computation.2 | loop fusion | flops 4194304 | bytes 12584960 | tf_op jit(solution)/shard_map/convert_element_type | solution.py:26
  52.3 23.8 %all_to_all.47 = bf16[4,512,512]{2,1,0:T(8,128)(2,1)S(1)} all-to-all(bf16[4,512,512]{2,1,0:T(8,128)(2,1)S(1)} %get-tuple-element.5), channel_id=1, replica_groups=mesh['fs'=4,'tp'=8] {'fs'}, dimensions={0} | all-to-all | bytes 4194304 | tf_op jit(solution)/shard_map/all_to_all | solution.py:29
  76.1 4.5 %all-to-all-start.2 = ((bf16[4,512,512]{2,1,0:T(8,128)(2,1)}), bf16[4,512,512]{2,1,0:T(8,128)(2,1)}, u32[]{:S(2)}, u32[]{:S(2)}) async-start(bf16[4,512,512]{2,1,0:T(8,128)(2,1)} %get-tuple-element.4), calls=%async_computation.2 | async-start | bytes 4194304 | tf_op jit(solution)/shard_map/all_to_all | solution.py:30
  80.6 3.8 %convert_element_type.47 = bf16[4,512,512]{2,1,0:T(8,128)(2,1)} convert(f32[4,512,512]{2,1,0:T(8,128)} %param.11) | non-fusion elementwise | flops 1048576 | bytes 6291456 | tf_op jit(solution)/shard_map/convert_element_type | solution.py:27
  84.4 16.0 %all-to-all-done.2 = bf16[4,512,512]{2,1,0:T(8,128)(2,1)} async-done(((bf16[4,512,512]{2,1,0:T(8,128)(2,1)}), bf16[4,512,512]{2,1,0:T(8,128)(2,1)}, u32[]{:S(2)}, u32[]{:S(2)}) %all-to-all-start.2) | async-done | bytes 2097184 | tf_op jit(solution)/shard_map/all_to_all | solution.py:30
  100.4 4.5 %all-to-all-start.3 = ((bf16[4,512,512]{2,1,0:T(8,128)(2,1)}), bf16[4,512,512]{2,1,0:T(8,128)(2,1)}, u32[]{:S(2)}, u32[]{:S(2)}) async-start(bf16[4,512,512]{2,1,0:T(8,128)(2,1)} %convert_element_type.47), calls=%async_computation.3 | async-start | bytes 4194304 | tf_op jit(solution)/shard_map/all_to_all | solution.py:31
  104.9 5.8 %fusion.5 = f32[1024,512]{1,0:T(8,128)} fusion(bf16[1024,2048]{1,0:T(8,128)(2,1)} %all-gather.2.cloned.1.call-done, bf16[2048,512]{1,0:T(8,128)(2,1)S(1)} %bitcast.28), kind=kOutput, calls=%fused_computation.28 | convolution fusion | flops 2147483648 | bytes 8388608 | tf_op jit(solution)/shard_map/dot_general | solution.py:55
  110.8 18.5 %all-to-all-done.3 = bf16[4,512,512]{2,1,0:T(8,128)(2,1)} async-done(((bf16[4,512,512]{2,1,0:T(8,128)(2,1)}), bf16[4,512,512]{2,1,0:T(8,128)(2,1)}, u32[]{:S(2)}, u32[]{:S(2)}) %all-to-all-start.3) | async-done | bytes 2097184 | tf_op jit(solution)/shard_map/all_to_all | solution.py:31
  129.3 10.6 %convert_bitcast_fusion = bf16[2048,1024]{0,1:T(8,128)(2,1)} fusion(bf16[2048,512]{1,0:T(8,128)(2,1)} %bitcast.9, f32[1024,512]{1,0:T(8,128)} %fusion.5, bf16[1024,2048]{1,0:T(8,128)(2,1)} %all-gather.2.cloned.1.call-done, bf16[2048,512]{1,0:T(8,128)(2,1)} %bitcast.8), kind=kOutput, calls=%fused_computation.1 | convolution fusion | flops 4300210176 | bytes 14680064 | tf_op jit(solution)/shard_map/dot_general | solution.py:60
  139.9 56.9 %reduce-scatter.2.cloned.1.call-done = bf16[256,1024]{0,1:T(8,128)(2,1)} async-done(((bf16[2048,1024]{0,1:T(8,128)(2,1)}), bf16[256,1024]{0,1:T(8,128)(2,1)}) %reduce-scatter.2.cloned.1.call-update) | async-done | bytes 524304 | tf_op jit(solution)/shard_map/reduce_scatter | solution.py:59
  196.8 4.1 %all-to-all-start.4 = ((bf16[256,4,256]{0,2,1:T(8,128)(2,1)}), bf16[256,4,256]{0,2,1:T(8,128)(2,1)}, u32[]{:S(2)}, u32[]{:S(2)}) async-start(bf16[256,4,256]{0,2,1:T(8,128)(2,1)} %bitcast.32), calls=%async_computation.5 | async-start | bytes 1048576 | tf_op jit(solution)/shard_map/all_to_all | solution.py:69
  201.0 0.3 select_reduce_fusion.1
  201.3 6.4 %all-to-all-done.4 = bf16[256,4,256]{0,2,1:T(8,128)(2,1)} async-done(((bf16[256,4,256]{0,2,1:T(8,128)(2,1)}), bf16[256,4,256]{0,2,1:T(8,128)(2,1)}, u32[]{:S(2)}, u32[]{:S(2)}) %all-to-all-start.4) | async-done | bytes 524320 | tf_op jit(solution)/shard_map/all_to_all | solution.py:69
  207.6 2.3 %convolution_convert_fusion = bf16[256,256]{1,0:T(8,128)(2,1)} fusion(f32[256,1024]{1,0:T(8,128)S(1)} %select_reduce_fusion.1, bf16[256,1024]{0,1:T(8,128)(2,1)} %bitcast.12), kind=kOutput, calls=%fused_computation.8 | convolution fusion | flops 805371904 | bytes 1703936 | tf_op jit(solution)/shard_map/dot_general | solution.py:72
  209.9 1.3 copy.26
  211.3 3.0 %copy.27 = bf16[1,2048,512]{2,1,0:T(8,128)(2,1)} copy(bf16[1,2048,512]{2,1,0:T(8,128)(2,1)} %bitcast.14) | data formatting | bytes 4194304
  214.3 3.0 %copy.28 = bf16[1,2048,512]{2,1,0:T(8,128)(2,1)} copy(bf16[1,2048,512]{2,1,0:T(8,128)(2,1)} %bitcast.15) | data formatting | bytes 4194304
  (21 shorter events, 0.3 us)
Async XLA Ops:
  7.2 97.8 %all-gather.2.cloned.1.call-start = ((), (), s32[]{:S(2)}) async-start(), calls=%async_computation.6 | async-start | bytes 4718592 | tf_op jit(solution)/shard_map/all_gather | solution.py:54
  31.4 14.7 %copy-start.1 = (f32[512]{0:T(512)S(1)}, f32[512]{0:T(512)}, u32[]{:S(2)}) copy-start(f32[512]{0:T(512)} %param.8) | copy-start | bytes 6148
  76.1 24.3 %all-to-all-start.2 = ((bf16[4,512,512]{2,1,0:T(8,128)(2,1)}), bf16[4,512,512]{2,1,0:T(8,128)(2,1)}, u32[]{:S(2)}, u32[]{:S(2)}) async-start(bf16[4,512,512]{2,1,0:T(8,128)(2,1)} %get-tuple-element.4), calls=%async_computation.2 | async-start | bytes 4194304 | tf_op jit(solution)/shard_map/all_to_all | solution.py:30
  100.4 28.9 %all-to-all-start.3 = ((bf16[4,512,512]{2,1,0:T(8,128)(2,1)}), bf16[4,512,512]{2,1,0:T(8,128)(2,1)}, u32[]{:S(2)}, u32[]{:S(2)}) async-start(bf16[4,512,512]{2,1,0:T(8,128)(2,1)} %convert_element_type.47), calls=%async_computation.3 | async-start | bytes 4194304 | tf_op jit(solution)/shard_map/all_to_all | solution.py:31
  104.9 92.0 %reduce-scatter.2.cloned.1.call-start = ((), (), s32[]{:S(2)}) async-start(), calls=%async_computation.7 | async-start | bytes 4718592 | tf_op jit(solution)/shard_map/reduce_scatter | solution.py:59
  139.9 61.1 %copy-start = (f32[256,2]{0,1:T(2,128)S(1)}, f32[256,2]{0,1:T(2,128)}, u32[]{:S(2)}) copy-start(f32[256,2]{0,1:T(2,128)} %param.13) | copy-start | bytes 6148
  196.8 10.8 %all-to-all-start.4 = ((bf16[256,4,256]{0,2,1:T(8,128)(2,1)}), bf16[256,4,256]{0,2,1:T(8,128)(2,1)}, u32[]{:S(2)}, u32[]{:S(2)}) async-start(bf16[256,4,256]{0,2,1:T(8,128)(2,1)} %bitcast.32), calls=%async_computation.5 | async-start | bytes 1048576 | tf_op jit(solution)/shard_map/all_to_all | solution.py:69
Sparse Core Ops, SparseCore 0:
  46.2 44.4 all-gather.1
  140.0 56.7 reduce-scatter.1
where the time goes:
time: 225 us; the launch traced here: 224 us
  waiting for transfers between devices  97.9 us (44%)
  blocking collectives  52.7 us (23%)
  matrix products  18.7 us (8%)
  other arithmetic  14.6 us (6%)
  between operations  14.2 us (6%)
  starting transfers between devices  13.2 us (6%)
  local copies, waits for them, and re-layouts  12.9 us (6%)
    reduce_scatter x1, waiting for transfers between devices, body(): lax.psum_scatter(lax.dot_general(down_local, hidden, (((1,), (1,)), ((),...  56.9 us
    all_to_all x1, blocking collectives, body(): lax.all_to_all(gate_cast, 'fs', split_axis=0, concat_axis=1, tiled=True)  23.8 us
    all_to_all x1, waiting for transfers between devices, body(): lax.all_to_all(down_cast, 'fs', split_axis=0, concat_axis=1, tiled=True)  18.5 us
    psum x1, blocking collectives, body(): square_sum = lax.psum(jnp.sum(tok_float * tok_float, axis=1), 'tp')  18.1 us
    all_to_all x1, waiting for transfers between devices, body(): lax.all_to_all(up_cast, 'fs', split_axis=0, concat_axis=1, tiled=True)  16 us
    all_to_all x1, blocking collectives, body(): lax.all_to_all(outgoing, 'fs', split_axis=0, concat_axis=0, tiled=True)  10.7 us
    dot_general x1, matrix products, body(): lax.dot_general(down_local, hidden, (((1,), (1,)), ((), ())), preferred_e...  10.6 us
    unnamed x8, local copies, waits for them, and re-layouts  8.23 us
  transfers between devices with their start and end apart: 5, of which 4 were waited for; matrix products, arithmetic and copies ran while one was open for 7% of the time, Pallas kernels for 0%

commit v1 on v0

--- a/solution.py
+++ b/solution.py
@@ -4,6 +4,14 @@
 from jax.sharding import PartitionSpec as P
 
 epsilon = 1e-05
+
+
+def extend_panels(s0, bus_axis):
+    t1 = jnp.concatenate(
+        lax.all_to_all(jnp.stack(jnp.split(s0, lax.axis_size(bus_axis), axis=0)), bus_axis, 0, 0),
+        axis=1,
+    )
+    return t1
 
 
 def slot_table(route, block_rows, expert_count):
@@ -28,7 +36,7 @@
     gate_new, up_new, down_new = (
         lax.all_to_all(gate_cast, "fs", split_axis=0, concat_axis=1, tiled=True),
         lax.all_to_all(up_cast, "fs", split_axis=0, concat_axis=1, tiled=True),
-        lax.all_to_all(down_cast, "fs", split_axis=0, concat_axis=1, tiled=True),
+        extend_panels(down_cast, "fs"),
     )
     slot_of = slot_table(route, tok_rows, experts)
     target = route * capacity + slot_of

time: 225 us -> 228 us (1.013)
  waiting for transfers between devices: 97.9 us -> 90.7 us
  blocking collectives: 52.7 us -> 58.3 us
  local copies, waits for them, and re-layouts: 12.9 us -> 16.9 us
    all_to_all x1, blocking collectives: 23.8 us -> 29.5 us  [body(): lax.all_to_all(gate_cast, 'fs', split_axis=0, concat_axis=1, tiled=True)]
    all_to_all x1, waiting for transfers between devices: 18.5 us -> 14.1 us  [extend_panels(): lax.all_to_all(jnp.stack(jnp.split(s0, lax.axis_size(bus_axis), axis=0)),...]
    reduce_scatter x1, waiting for transfers between devices: 56.9 us -> 53.7 us  [body(): lax.psum_scatter(lax.dot_general(down_local, hidden, (((1,), (1,)), ((),...]
  transfers between devices with their start and end apart: 5 -> 5, of which waited for: 4 -> 4; matrix products, arithmetic and copies ran while one was open for 7% -> 8% of each run, Pallas kernels for 0% -> 0%
where the time goes in v1:
time: 228 us; the launch traced here: 227 us
  waiting for transfers between devices  90.7 us (40%)
  blocking collectives  58.3 us (26%)
  matrix products  18.9 us (8%)
  local copies, waits for them, and re-layouts  16.9 us (7%)
  other arithmetic  15.5 us (7%)
  between operations  14.2 us (6%)
  starting transfers between devices  12.5 us (5%)
    reduce_scatter x1, waiting for transfers between devices, body(): lax.psum_scatter(lax.dot_general(down_local, hidden, (((1,), (1,)), ((),...  53.7 us
    all_to_all x1, blocking collectives, body(): lax.all_to_all(gate_cast, 'fs', split_axis=0, concat_axis=1, tiled=True)  29.5 us
    psum x1, blocking collectives, body(): square_sum = lax.psum(jnp.sum(tok_float * tok_float, axis=1), 'tp')  18.1 us
    all_to_all x1, waiting for transfers between devices, body(): lax.all_to_all(up_cast, 'fs', split_axis=0, concat_axis=1, tiled=True)  16.6 us
    all_to_all x1, waiting for transfers between devices, extend_panels(): lax.all_to_all(jnp.stack(jnp.split(s0, lax.axis_size(bus_axis), axis=0)),...  14.1 us
    all_to_all x1, blocking collectives, body(): lax.all_to_all(outgoing, 'fs', split_axis=0, concat_axis=0, tiled=True)  10.7 us
    dot_general x1, matrix products, body(): lax.dot_general(down_local, hidden, (((1,), (1,)), ((), ())), preferred_e...  10.1 us
    unnamed x8, local copies, waits for them, and re-layouts  8.23 us
  transfers between devices with their start and end apart: 5, of which 4 were waited for; matrix products, arithmetic and copies ran while one was open for 8% of the time, Pallas kernels for 0%

profile of v1, /device:TPU:0, one launch (start us, length us, event | category | flops | bytes accessed | tf_op | source)
XLA Modules:
  0.0 227.1 jit_solution(15596830270283513134)
XLA Ops:
  7.2 0.8 copy.34
  8.0 0.1 eq.40
  8.2 1.2 reduce-window.6
  9.4 0.2 slice_reduce_fusion
  9.7 0.2 reduce-window.9
  10.2 0.7 multiply_add_fusion
  10.9 0.3 select_reduce_fusion
  11.2 1.0 fusion
  12.2 18.1 %psum.7 = f32[256]{0:T(256)S(1)} all-reduce(f32[256]{0:T(256)S(1)} %fusion), channel_id=1, replica_groups=mesh['fs'=4,'tp'=8] {'tp'}, use_global_device_ids=true, to_apply=%region_5.6 | all-reduce | flops 256 | bytes 2048 | tf_op jit(solution)/shard_map/psum | solution.py:50
  30.4 1.0 fusion.1
  31.4 3.9 %gather_fusion = bf16[1024,256]{1,0:T(8,128)(2,1)S(1)} fusion(bf16[257,256]{1,0:T(8,128)(2,1)S(1)} %concatenate.3, s32[1024]{0:T(1024)S(1)} %broadcast_clamp_fusion), kind=kCustom, calls=%fused_computation | custom fusion | bytes 1052672 | tf_op jit(solution)/shard_map/gather | solution.py:56
  35.3 10.7 %all_to_all.39 = bf16[4,256,256]{2,1,0:T(8,128)(2,1)} all-to-all(bf16[4,256,256]{2,1,0:T(8,128)(2,1)S(1)} %bitcast.43), channel_id=1, replica_groups=mesh['fs'=4,'tp'=8] {'fs'}, dimensions={0} | all-to-all | bytes 1048576 | tf_op jit(solution)/shard_map/all_to_all | solution.py:57
  46.1 2.5 %convert_element_type.39 = bf16[4,512,512]{2,1,0:T(8,128)(2,1)S(1)} convert(f32[4,512,512]{2,1,0:T(8,128)} %param.11) | non-fusion elementwise | flops 1048576 | bytes 6291456 | tf_op jit(solution)/shard_map/convert_element_type | solution.py:35
  48.7 1.6 pad_maximum_fusion
  50.3 3.8 %all-to-all-start = ((bf16[4,1,512,512]{3,2,1,0:T(8,128)(2,1)}), bf16[4,1,512,512]{3,2,1,0:T(8,128)(2,1)S(1)}, u32[]{:S(2)}, u32[]{:S(2)}) async-start(bf16[4,1,512,512]{3,2,1,0:T(8,128)(2,1)} %pad_maximum_fusion), calls=%async_computation | async-start | bytes 4194304 | tf_op jit(solution)/shard_map/all_to_all | solution.py:11
  54.1 6.8 %multiply_convert_fusion = (bf16[4,512,512]{2,1,0:T(8,128)(2,1)}, bf16[4,512,512]{2,1,0:T(8,128)(2,1)}) fusion(f32[4,512,512]{2,1,0:T(8,128)} %param.10, f32[512]{0:T(512)S(1)} %copy-done.1, f32[4,512,512]{2,1,0:T(8,128)} %param.9), kind=kLoop, calls=%fused_computation.1 | loop fusion | flops 4194304 | bytes 12584960 | tf_op jit(solution)/shard_map/convert_element_type | solution.py:34
  60.8 14.1 %all-to-all-done = bf16[4,1,512,512]{3,2,1,0:T(8,128)(2,1)S(1)} async-done(((bf16[4,1,512,512]{3,2,1,0:T(8,128)(2,1)}), bf16[4,1,512,512]{3,2,1,0:T(8,128)(2,1)S(1)}, u32[]{:S(2)}, u32[]{:S(2)}) %all-to-all-start) | async-done | bytes 2097184 | tf_op jit(solution)/shard_map/all_to_all | solution.py:11
  74.9 29.5 %all_to_all.40 = bf16[4,512,512]{2,1,0:T(8,128)(2,1)} all-to-all(bf16[4,512,512]{2,1,0:T(8,128)(2,1)} %get-tuple-element.9), channel_id=1, replica_groups=mesh['fs'=4,'tp'=8] {'fs'}, dimensions={0} | all-to-all | bytes 4194304 | tf_op jit(solution)/shard_map/all_to_all | solution.py:37
  104.4 4.5 %all-to-all-start.3 = ((bf16[4,512,512]{2,1,0:T(8,128)(2,1)}), bf16[4,512,512]{2,1,0:T(8,128)(2,1)}, u32[]{:S(2)}, u32[]{:S(2)}) async-start(bf16[4,512,512]{2,1,0:T(8,128)(2,1)} %get-tuple-element.8), calls=%async_computation.3 | async-start | bytes 4194304 | tf_op jit(solution)/shard_map/all_to_all | solution.py:38
  109.0 6.5 %fusion.5 = f32[1024,512]{1,0:T(8,128)} fusion(bf16[1024,2048]{1,0:T(8,128)(2,1)} %all-gather.2.cloned.1.call-done, bf16[2048,512]{1,0:T(8,128)(2,1)} %bitcast.39), kind=kOutput, calls=%fused_computation.34 | convolution fusion | flops 2147483648 | bytes 8388608 | tf_op jit(solution)/shard_map/dot_general | solution.py:63
  115.5 16.6 %all-to-all-done.3 = bf16[4,512,512]{2,1,0:T(8,128)(2,1)} async-done(((bf16[4,512,512]{2,1,0:T(8,128)(2,1)}), bf16[4,512,512]{2,1,0:T(8,128)(2,1)}, u32[]{:S(2)}, u32[]{:S(2)}) %all-to-all-start.3) | async-done | bytes 2097184 | tf_op jit(solution)/shard_map/all_to_all | solution.py:38
  132.0 10.1 %convolution_convert_fusion = bf16[2048,1024]{1,0:T(8,128)(2,1)} fusion(bf16[2048,512]{1,0:T(8,128)(2,1)S(1)} %bitcast.37, f32[1024,512]{1,0:T(8,128)} %fusion.5, bf16[1024,2048]{1,0:T(8,128)(2,1)} %all-gather.2.cloned.1.call-done, bf16[2048,512]{1,0:T(8,128)(2,1)} %bitcast.13), kind=kOutput, calls=%fused_computation.3 | convolution fusion | flops 4300210176 | bytes 14680064 | tf_op jit(solution)/shard_map/dot_general | solution.py:68
  142.2 53.7 %reduce-scatter.2.cloned.1.call-done = bf16[256,1024]{1,0:T(8,128)(2,1)} async-done(((bf16[2048,1024]{1,0:T(8,128)(2,1)}), bf16[256,1024]{1,0:T(8,128)(2,1)}) %reduce-scatter.2.cloned.1.call-update) | async-done | bytes 524304 | tf_op jit(solution)/shard_map/reduce_scatter | solution.py:67
  195.8 1.9 copy.40
  197.7 4.1 %all-to-all-start.4 = ((bf16[256,4,256]{2,0,1:T(8,128)(2,1)}), bf16[256,4,256]{2,0,1:T(8,128)(2,1)}, u32[]{:S(2)}, u32[]{:S(2)}) async-start(bf16[256,4,256]{2,0,1:T(8,128)(2,1)} %bitcast.36), calls=%async_computation.5 | async-start | bytes 1048576 | tf_op jit(solution)/shard_map/all_to_all | solution.py:77
  201.9 0.3 select_reduce_fusion.1
  202.1 6.4 %all-to-all-done.4 = bf16[256,4,256]{2,0,1:T(8,128)(2,1)} async-done(((bf16[256,4,256]{2,0,1:T(8,128)(2,1)}), bf16[256,4,256]{2,0,1:T(8,128)(2,1)}, u32[]{:S(2)}, u32[]{:S(2)}) %all-to-all-start.4) | async-done | bytes 524320 | tf_op jit(solution)/shard_map/all_to_all | solution.py:77
  208.5 2.0 copy.37
  210.5 2.3 %convolution_convert_fusion.1 = bf16[256,256]{1,0:T(8,128)(2,1)} fusion(f32[256,1024]{1,0:T(8,128)S(1)} %select_reduce_fusion.1, bf16[256,1024]{0,1:T(8,128)(2,1)} %bitcast.42), kind=kOutput, calls=%fused_computation.9 | convolution fusion | flops 805371904 | bytes 1703936 | tf_op jit(solution)/shard_map/dot_general | solution.py:80
  212.8 3.0 %copy.44 = bf16[1,2048,512]{2,1,0:T(8,128)(2,1)} copy(bf16[1,2048,512]{2,1,0:T(8,128)(2,1)} %bitcast.40) | data formatting | bytes 4194304
  215.9 3.0 %copy.45 = bf16[1,2048,512]{2,1,0:T(8,128)(2,1)} copy(bf16[1,2048,512]{2,1,0:T(8,128)(2,1)} %bitcast.16) | data formatting | bytes 4194304
  218.9 1.3 copy.46
  (25 shorter events, 0.7 us)
Async XLA Ops:
  7.2 101.8 %all-gather.2.cloned.1.call-start = ((), (), s32[]{:S(2)}) async-start(), calls=%async_computation.6 | async-start | bytes 4718592 | tf_op jit(solution)/shard_map/all_gather | solution.py:62
  50.3 3.8 %copy-start.1 = (f32[512]{0:T(512)S(1)}, f32[512]{0:T(512)}, u32[]{:S(2)}) copy-start(f32[512]{0:T(512)} %param.8) | copy-start | bytes 6148
  50.3 24.6 %all-to-all-start = ((bf16[4,1,512,512]{3,2,1,0:T(8,128)(2,1)}), bf16[4,1,512,512]{3,2,1,0:T(8,128)(2,1)S(1)}, u32[]{:S(2)}, u32[]{:S(2)}) async-start(bf16[4,1,512,512]{3,2,1,0:T(8,128)(2,1)} %pad_maximum_fusion), calls=%async_computation | async-start | bytes 4194304 | tf_op jit(solution)/shard_map/all_to_all | solution.py:11
  104.4 27.6 %all-to-all-start.3 = ((bf16[4,512,512]{2,1,0:T(8,128)(2,1)}), bf16[4,512,512]{2,1,0:T(8,128)(2,1)}, u32[]{:S(2)}, u32[]{:S(2)}) async-start(bf16[4,512,512]{2,1,0:T(8,128)(2,1)} %get-tuple-element.8), calls=%async_computation.3 | async-start | bytes 4194304 | tf_op jit(solution)/shard_map/all_to_all | solution.py:38
  108.9 86.9 %reduce-scatter.2.cloned.1.call-start = ((), (), s32[]{:S(2)}) async-start(), calls=%async_computation.7 | async-start | bytes 4718592 | tf_op jit(solution)/shard_map/reduce_scatter | solution.py:67
  142.1 59.7 %copy-start = (f32[256,2]{0,1:T(2,128)S(1)}, f32[256,2]{0,1:T(2,128)}, u32[]{:S(2)}) copy-start(f32[256,2]{0,1:T(2,128)} %param.13) | copy-start | bytes 6148
  197.7 10.8 %all-to-all-start.4 = ((bf16[256,4,256]{2,0,1:T(8,128)(2,1)}), bf16[256,4,256]{2,0,1:T(8,128)(2,1)}, u32[]{:S(2)}, u32[]{:S(2)}) async-start(bf16[256,4,256]{2,0,1:T(8,128)(2,1)} %bitcast.36), calls=%async_computation.5 | async-start | bytes 1048576 | tf_op jit(solution)/shard_map/all_to_all | solution.py:77
Sparse Core Ops, SparseCore 0:
  46.2 44.4 all-gather.1
  142.3 53.5 reduce-scatter.1
